TPU v7x, 512 devices: a 4x2x32 block of a 4x8x32 slice. The times are simulated.
512 devices in a mesh: grp: 2 (over y), fs: 32 (over z), tp: 8 (over x, core).
Axes of the slice: x: 4, y: 2, z: 32, core: 2. Of those that a mesh axis runs over, the one named last changes fastest.
The devices are a block of a 4x8x32 slice.
Arguments:
- tokens: bfloat16 [64, 384, 2048], P(('grp', 'fs'), None, 'tp'), parts along dimension 0, may hold values from -24 to 24
- input_gain: float32 [2048], replicated, may hold values from 0.1 to 1.9
- query_weight: bfloat16 [2048, 1024], P('fs', 'tp'), may hold values from -0.125 to 0.125
- key_weight: bfloat16 [2048, 1024], P('fs', 'tp'), may hold values from -0.125 to 0.125
- value_weight: bfloat16 [2048, 1024], P('fs', 'tp'), may hold values from -0.125 to 0.125
- output_gate_matrix: bfloat16 [2048, 1024], P('fs', 'tp'), may hold values from -0.125 to 0.125
- forward_decay: float32 [16], P('tp'), may hold values from -1 to 9
- backward_decay: float32 [16], P('tp'), may hold values from -1 to 9
- merge_weight: bfloat16 [1024, 2048], P('tp', 'fs'), may hold values from -0.375 to 0.375
- middle_gain: float32 [2048], replicated, may hold values from 0.1 to 1.9
- gate_weight: bfloat16 [2048, 5120], P('fs', 'tp'), may hold values from -0.125 to 0.125
- up_weight: bfloat16 [2048, 5120], P('fs', 'tp'), may hold values from -0.125 to 0.125
- down_weight: bfloat16 [5120, 2048], P('tp', 'fs'), may hold values from -0.15625 to 0.15625
Outputs:
- layer_out: bfloat16 [64, 384, 2048], P(('grp', 'fs'), None, 'tp'), parts along dimension 0
There are 2 independent parts, one for each index of `grp`. A program takes and returns all parts, laid end to end along the dimension named above; an argument that names none is the same for every part. Nothing has to cross between parts.
All inputs are finite; a program needn't handle non-finite values.
Results may differ from a plain program's by a relative error of at most 0.019.
Values may be sent and summed in bfloat16 or wider, within the bound.
A program may use at most 64 MiB of HBM per device.

v0:
```python
import jax
import jax.numpy as jnp
from jax import lax
from jax.sharding import PartitionSpec as P

BLOCK = 128
norm_eps = 1e-06
group_eps = 1e-05
rope_base = 10000.0
highest_precision = lax.Precision.HIGHEST


def joined_along(tiles, dim):
    tiles = jnp.moveaxis(tiles, 0, dim)
    lengths = tiles.shape
    return tiles.reshape(*lengths[:dim], lengths[dim] * lengths[dim + 1], *lengths[dim + 2 :])


def copy_for_each(array, axis):
    copies = jnp.broadcast_to(array, (lax.axis_size(axis), *array.shape))
    return lax.all_to_all(copies, axis, split_axis=0, concat_axis=0, tiled=True)


def gathered_copies(array, axis, dim):
    return joined_along(copy_for_each(array, axis), dim)


def sent_together(arrays, axis, dim, along):
    both = jnp.concatenate(arrays, axis=along)
    result, at, gathered = (lax.all_gather(both, axis, axis=dim, tiled=True), 0, [])
    for a in arrays:
        gathered.append(lax.slice_in_dim(result, at, at + a.shape[along], axis=along))
        at += a.shape[along]
    return tuple(gathered)


def split_up(array, dim, peers):
    lengths = array.shape
    tiles = array.reshape(*lengths[:dim], peers, lengths[dim] // peers, *lengths[dim + 1 :])
    return jnp.moveaxis(tiles, dim, 0)


def summed_on_arrival(array, axis, dim):
    peers = lax.axis_size(axis)
    tiles = lax.all_to_all(split_up(array, dim, peers), axis, 0, 0, tiled=True)
    return jnp.sum(tiles.astype(jnp.float32), axis=0)


def rms_scale(values, gain_vector):
    widened = values.astype(jnp.float32)
    scaled = widened * lax.rsqrt(jnp.mean(widened * widened, axis=-1, keepdims=True) + norm_eps)
    return (scaled * gain_vector).astype(jnp.bfloat16)


def apply_rotary_heads(values, length):
    half_dim = values.shape[-1] // 2
    inverse = rope_base ** (-jnp.arange(half_dim, dtype=jnp.float32) / half_dim)
    angles = jnp.arange(length, dtype=jnp.float32)[:, None] * inverse[None, :]
    cosine = jnp.cos(angles)[:, None, :]
    sine_part = jnp.sin(angles)[:, None, :]
    lower_half = values[..., :half_dim]
    upper_half = values[..., half_dim:]
    return jnp.concatenate(
        [
            lower_half * cosine - upper_half * sine_part,
            upper_half * cosine + lower_half * sine_part,
        ],
        axis=-1,
    )


def carry_states(key_blocks, value_blocks, weighting, log_rates, block_size, backward):
    block_terms = jnp.einsum(
        "sbmhd,sbmhe->bshde",
        key_blocks * weighting[None, None, :, :, None],
        value_blocks,
        precision=highest_precision,
    )
    factor = jnp.exp(log_rates * block_size)[None, :, None, None]

    def advance(running, addend):
        return (running * factor + addend, running)

    initial = jnp.zeros(block_terms.shape[1:], jnp.float32)
    return lax.scan(advance, initial, block_terms, reverse=backward)[1]


def retain_blocks(
    query_rows, key_rows, value_rows, gate_rows, forward_decay, backward_decay, seq_count, length
):
    head_count = forward_decay.shape[0]
    head_dim = query_rows.shape[1] // head_count
    block_size = BLOCK
    block_count = length // block_size

    def split_heads(rows_in):
        return rows_in.astype(jnp.float32).reshape(seq_count, length, head_count, head_dim)

    def blocked(tensor):
        return tensor.reshape(seq_count, block_count, block_size, head_count, head_dim)

    queries = blocked(apply_rotary_heads(split_heads(query_rows), length))
    key_heads = blocked(apply_rotary_heads(split_heads(key_rows), length) * head_dim ** (-0.5))
    valued = blocked(split_heads(value_rows))
    rate_ahead = jax.nn.log_sigmoid(forward_decay)
    rate_behind = jax.nn.log_sigmoid(backward_decay)
    position = jnp.arange(block_size, dtype=jnp.float32)
    offset = position[:, None] - position[None, :]
    inside = jnp.where(
        offset[None] >= 0,
        jnp.exp(rate_ahead[:, None, None] * jnp.maximum(offset, 0.0)[None]),
        jnp.exp(rate_behind[:, None, None] * jnp.maximum(-offset, 0.0)[None]),
    )
    attention_scores = (
        jnp.einsum("sbchd,sbmhd->sbhcm", queries, key_heads, precision=highest_precision)
        * inside[None, None]
    )
    result = jnp.einsum("sbhcm,sbmhd->sbchd", attention_scores, valued, precision=highest_precision)
    column = position[:, None]
    key_ahead = jnp.exp(rate_ahead[None, :] * (block_size - 1 - column))
    query_ahead = jnp.exp(rate_ahead[None, :] * (column + 1))
    key_behind = jnp.exp(rate_behind[None, :] * column)
    query_behind = jnp.exp(rate_behind[None, :] * (block_size - column))
    from_before = carry_states(key_heads, valued, key_ahead, rate_ahead, block_size, False)
    from_after = carry_states(key_heads, valued, key_behind, rate_behind, block_size, True)
    result = (
        result
        + jnp.einsum("sbchd,bshde->sbche", queries, from_before, precision=highest_precision)
        * query_ahead[None, None, :, :, None]
    )
    result = (
        result
        + jnp.einsum("sbchd,bshde->sbche", queries, from_after, precision=highest_precision)
        * query_behind[None, None, :, :, None]
    )
    result = result.reshape(seq_count, length, head_count, head_dim)
    center = jnp.mean(result, axis=-1, keepdims=True)
    spread = jnp.mean(jnp.square(result - center), axis=-1, keepdims=True)
    normalized = (result - center) * lax.rsqrt(spread + group_eps)
    gated = jax.nn.silu(split_heads(gate_rows)) * normalized
    return gated.reshape(seq_count * length, head_count * head_dim).astype(jnp.bfloat16)


def accumulate(pieces, source):
    return tuple(
        (
            jnp.dot(source, weight_piece, preferred_element_type=jnp.float32)
            for weight_piece in pieces
        )
    )


def on_device(
    tokens,
    input_gain,
    query_weight,
    key_weight,
    value_weight,
    output_gate_matrix,
    forward_decay,
    backward_decay,
    merge_weight,
    middle_gain,
    gate_weight,
    up_weight,
    down_weight,
):
    seq_count, length, part_width = tokens.shape
    row_count = seq_count * length
    gathered = gathered_copies(tokens, "tp", 2)
    normed = rms_scale(gathered.reshape(row_count, gathered.shape[2]), input_gain)
    query_sum, key_sum, value_sum, gating_sum = accumulate(
        sent_together((query_weight, key_weight, value_weight, output_gate_matrix), "fs", 0, 1),
        normed,
    )
    mixed = retain_blocks(
        query_sum.astype(jnp.bfloat16),
        key_sum.astype(jnp.bfloat16),
        value_sum.astype(jnp.bfloat16),
        gating_sum.astype(jnp.bfloat16),
        forward_decay,
        backward_decay,
        seq_count,
        length,
    )
    merge_term = jnp.dot(
        mixed,
        lax.all_gather(merge_weight, "fs", axis=1, tiled=True),
        preferred_element_type=jnp.float32,
    )
    merged = summed_on_arrival(merge_term.astype(jnp.bfloat16), "tp", 1)
    middle = (tokens.reshape(row_count, part_width).astype(jnp.float32) + merged).astype(
        jnp.bfloat16
    )
    gathered_mid = gathered_copies(middle, "tp", 1)
    normed_mid = rms_scale(gathered_mid, middle_gain)
    gate_full, up_full = sent_together((gate_weight, up_weight), "fs", 0, 1)
    gate_act = jnp.dot(normed_mid, gate_full, preferred_element_type=jnp.float32)
    up_act = jnp.dot(normed_mid, up_full, preferred_element_type=jnp.float32)
    hidden = (jax.nn.silu(gate_act) * up_act).astype(jnp.bfloat16)
    down_term = jnp.dot(
        hidden,
        lax.all_gather(down_weight, "fs", axis=1, tiled=True),
        preferred_element_type=jnp.float32,
    )
    summed = summed_on_arrival(down_term.astype(jnp.bfloat16), "tp", 1)
    layer_out = (middle.astype(jnp.float32) + summed).astype(jnp.bfloat16)
    return layer_out.reshape(seq_count, length, part_width)


def solution(mesh):
    placed = (
        P(("grp", "fs"), None, "tp"),
        P(),
        P("fs", "tp"),
        P("fs", "tp"),
        P("fs", "tp"),
        P("fs", "tp"),
        P("tp"),
        P("tp"),
        P("tp", "fs"),
        P(),
        P("fs", "tp"),
        P("fs", "tp"),
        P("tp", "fs"),
    )
    return jax.shard_map(
        on_device,
        mesh=mesh,
        in_specs=placed,
        out_specs=P(("grp", "fs"), None, "tp"),
        check_vma=False,
    )
```

profile of v0, /device:TPU:33, one launch (start us, length us, event | category | flops | bytes accessed | tf_op | source)
XLA Modules:
  0.0 478.5 jit_solution(4488102892256830335)
XLA Ops:
  6.6 1.4 pad_maximum_fusion.2
  8.1 1.6 pad_maximum_fusion.1
  9.8 1.1 copy.41
  10.9 1.3 broadcast_in_dim.28
  12.1 45.1 %all-to-all-start = ((bf16[8,1,384,256]{2,3,1,0:T(8,128)(2,1)}), bf16[8,1,384,256]{2,3,1,0:T(8,128)(2,1)S(1)}, u32[]{:S(2)}, u32[]{:S(2)}) async-start(bf16[8,1,384,256]{2,3,1,0:T(8,128)(2,1)} %broadcast_in_dim.28), calls=%async_computation | async-start | bytes 3145728 | tf_op jit(solution)/shard_map/all_to_all | solution.py:21
  57.2 0.7 all-gather.8.cloned.1.call-update
  58.7 51.9 %all_gather.13 = bf16[128,2048]{0,1:T(8,128)(2,1)} all-gather(bf16[128,64]{0,1:T(8,128)(2,1)S(1)} %copy-done.2), channel_id=1, replica_groups=mesh['grp'=2,'fs'=32,'tp'=8] {'fs'}, dimensions={1}, use_global_device_ids=true | all-gather | bytes 540672 | tf_op jit(solution)/shard_map/all_gather | solution.py:188
  110.6 0.4 multiply_reduce_fusion.1
  111.3 0.5 copy-done.3
  111.8 0.4 fusion.3
  112.1 38.8 %all-gather.4.cloned.1.call-done = bf16[2048,512]{1,0:T(8,128)(2,1)} async-done(((bf16[64,512]{1,0:T(8,128)(2,1)}), bf16[2048,512]{1,0:T(8,128)(2,1)}) %all-gather.4.cloned.1.call-update) | async-done | bytes 2097168 | tf_op jit(solution)/shard_map/all_gather | solution.py:30
  150.9 1.5 convolution_convert_fusion.3
  152.5 1.5 convolution_convert_fusion.2
  154.2 1.7 convolution_convert_fusion.4
  156.5 0.3 while.30
  157.2 0.3 while.31
  157.5 0.8 convolution_multiply_fusion
  158.3 0.5 fusion.16
  158.8 0.5 fusion.17
  159.3 0.5 fusion.56
  160.0 0.9 reshape.439
  161.3 3.2 convolution_convert_fusion.1
  164.6 46.3 %all_to_all.20 = bf16[8,384,256]{2,1,0:T(8,128)(2,1)S(1)} all-to-all(bf16[8,384,256]{2,1,0:T(8,128)(2,1)S(1)} %bitcast.140), channel_id=1, replica_groups=mesh['grp'=2,'fs'=32,'tp'=8] {'tp'}, dimensions={0} | all-to-all | bytes 3145728 | tf_op jit(solution)/shard_map/all_to_all | solution.py:45
  211.5 24.2 %all_to_all.21 = bf16[8,384,256]{1,2,0:T(8,128)(2,1)S(1)} all-to-all(bf16[8,384,256]{1,2,0:T(8,128)(2,1)S(1)} %broadcast_in_dim.33), channel_id=1, replica_groups=mesh['grp'=2,'fs'=32,'tp'=8] {'tp'}, dimensions={0} | all-to-all | bytes 3145728 | tf_op jit(solution)/shard_map/all_to_all | solution.py:21
  235.7 0.4 multiply_reduce_fusion
  236.1 0.4 fusion.1
  236.5 52.4 %all-gather.6.cloned.1.call-done = bf16[2048,1280]{1,0:T(8,128)(2,1)} async-done(((bf16[64,1280]{1,0:T(8,128)(2,1)}), bf16[2048,1280]{1,0:T(8,128)(2,1)}) %all-gather.6.cloned.1.call-update) | async-done | bytes 5242896 | tf_op jit(solution)/shard_map/all_gather | solution.py:30
  288.9 3.2 fusion.6
  292.1 126.9 %all-gather.8.cloned.1.call-done = bf16[640,2048]{0,1:T(8,128)(2,1)} async-done(((bf16[640,64]{0,1:T(8,128)(2,1)}), bf16[640,2048]{0,1:T(8,128)(2,1)}) %all-gather.8.cloned.1.call-update) | async-done | bytes 2621456 | tf_op jit(solution)/shard_map/all_gather | solution.py:203
  419.0 6.2 %convolution_convert_fusion = bf16[384,2048]{1,0:T(8,128)(2,1)S(1)} fusion(bf16[640,2048]{0,1:T(8,128)(2,1)} %all-gather.8.cloned.1.call-done, bf16[384,2048]{0,1:T(8,128)(2,1)} %copy-done.1, bf16[2048,1280]{1,0:T(8,128)(2,1)} %all-gather.6.cloned.1.call-done, f32[384,640]{1,0:T(8,128)S(1)} %fusion.6), kind=kOutput, calls=%fused_computation.14 | convolution fusion | flops 2015526912 | bytes 9371648 | tf_op jit(solution)/shard_map/dot_general | solution.py:201
  425.3 45.7 %all_to_all.22 = bf16[8,384,256]{2,1,0:T(8,128)(2,1)S(1)} all-to-all(bf16[8,384,256]{2,1,0:T(8,128)(2,1)S(1)} %bitcast.141), channel_id=1, replica_groups=mesh['grp'=2,'fs'=32,'tp'=8] {'tp'}, dimensions={0} | all-to-all | bytes 3145728 | tf_op jit(solution)/shard_map/all_to_all | solution.py:45
  471.2 0.8 fusion.26
  (76 shorter events, 4.3 us)
Async XLA Ops:
  6.5 144.4 %all-gather.4.cloned.1.call-start = ((), (), s32[]{:S(2)}) async-start(), calls=%async_computation.4 | async-start | bytes 2162688 | tf_op jit(solution)/shard_map/all_gather | solution.py:30
  8.0 280.9 %all-gather.6.cloned.1.call-start = ((), (), s32[]{:S(2)}) async-start(), calls=%async_computation.5 | async-start | bytes 5406720 | tf_op jit(solution)/shard_map/all_gather | solution.py:30
  12.1 46.0 %copy-start.5 = (f32[2]{0:T(128)S(1)}, f32[2]{0:T(128)}, u32[]{:S(2)}) copy-start(f32[2]{0:T(128)} %param.24) | copy-start | bytes 28
  12.1 46.0 %copy-start.6 = (f32[2]{0:T(128)S(1)}, f32[2]{0:T(128)}, u32[]{:S(2)}) copy-start(f32[2]{0:T(128)} %param.23) | copy-start | bytes 28
  12.1 46.5 %copy-start.2 = (bf16[128,64]{0,1:T(8,128)(2,1)S(1)}, bf16[128,64]{0,1:T(8,128)(2,1)}, u32[]{:S(2)}) copy-start(bf16[128,64]{0,1:T(8,128)(2,1)} %param.25) | copy-start | bytes 49156
  12.1 98.5 %all-to-all-start = ((bf16[8,1,384,256]{2,3,1,0:T(8,128)(2,1)}), bf16[8,1,384,256]{2,3,1,0:T(8,128)(2,1)S(1)}, u32[]{:S(2)}, u32[]{:S(2)}) async-start(bf16[8,1,384,256]{2,3,1,0:T(8,128)(2,1)} %broadcast_in_dim.28), calls=%async_computation | async-start | bytes 3145728 | tf_op jit(solution)/shard_map/all_to_all | solution.py:21
  57.2 361.8 %all-gather.8.cloned.1.call-start = ((), (), s32[]{:S(2)}) async-start(), calls=%async_computation.6 | async-start | bytes 2703360 | tf_op jit(solution)/shard_map/all_gather | solution.py:203
  111.1 0.7 copy-start.3
  164.6 46.5 %copy-start = (bf16[1,384,256]{2,1,0:T(8,128)(2,1)S(1)}, bf16[1,384,256]{2,1,0:T(8,128)(2,1)}, u32[]{:S(2)}) copy-start(bf16[1,384,256]{2,1,0:T(8,128)(2,1)} %param.17) | copy-start | bytes 589828
  211.5 24.6 %copy-start.4 = (f32[2048]{0:T(1024)S(1)}, f32[2048]{0:T(1024)}, u32[]{:S(2)}) copy-start(f32[2048]{0:T(1024)} %param.26) | copy-start | bytes 24580
  236.5 55.6 %copy-start.1 = (bf16[384,2048]{0,1:T(8,128)(2,1)}, bf16[384,2048]{0,1:T(8,128)(2,1)S(1)}, u32[]{:S(2)}) copy-start(bf16[384,2048]{0,1:T(8,128)(2,1)S(1)} %fusion.1) | copy-start | bytes 4718596
Sparse Core Ops, SparseCore 0:
  9.4 141.4 all-gather.3
  153.0 135.8 all-gather.5
  291.0 127.9 all-gather.7
where the time goes:
time: 479 us
  waiting for transfers between devices  219 us (46%)
  blocking collectives  168 us (35%)
  starting transfers between devices  45.1 us (9%)
  matrix products  20.1 us (4%)
  between operations  13.6 us (3%)
  other arithmetic  7.42 us (2%)
  local copies, waits for them, and re-layouts  5.26 us (1%)
    all_gather x1, waiting for transfers between devices, on_device(): lax.all_gather(down_weight, 'fs', axis=1, tiled=True)  127 us
    all_to_all x2, blocking collectives, summed_on_arrival(): tiles = lax.all_to_all(split_up(array, dim, peers), axis, 0, 0, tiled=True)  92 us
    all_gather x2, waiting for transfers between devices, sent_together(): lax.all_gather(both, axis, axis=dim, tiled=True)  91.2 us
    all_gather x1, blocking collectives, on_device(): lax.all_gather(merge_weight, 'fs', axis=1, tiled=True)  51.9 us
    all_to_all x1, starting transfers between devices, copy_for_each(): return lax.all_to_all(copies, axis, split_axis=0, concat_axis=0, tiled=True)  45.1 us
    all_to_all x1, blocking collectives, copy_for_each(): return lax.all_to_all(copies, axis, split_axis=0, concat_axis=0, tiled=True)  24.2 us
  transfers between devices with their start and end apart: 4, of which 3 were waited for; matrix products, arithmetic and copies ran while one was open for 5% of the time, Pallas kernels for 0%

commit v1 on v0

--- a/solution.py
+++ b/solution.py
@@ -8,6 +8,12 @@
 group_eps = 1e-05
 rope_base = 10000.0
 highest_precision = lax.Precision.HIGHEST
+
+
+def _change_members_all(v0):
+    return jnp.concatenate(
+        lax.all_to_all(jnp.stack([v0] * lax.axis_size("fs"), axis=0), "fs", 0, 0), 1
+    )
 
 
 def joined_along(tiles, dim):
@@ -199,9 +205,7 @@
     up_act = jnp.dot(normed_mid, up_full, preferred_element_type=jnp.float32)
     hidden = (jax.nn.silu(gate_act) * up_act).astype(jnp.bfloat16)
     down_term = jnp.dot(
-        hidden,
-        lax.all_gather(down_weight, "fs", axis=1, tiled=True),
-        preferred_element_type=jnp.float32,
+        hidden, _change_members_all(down_weight), preferred_element_type=jnp.float32
     )
     summed = summed_on_arrival(down_term.astype(jnp.bfloat16), "tp", 1)
     layer_out = (middle.astype(jnp.float32) + summed).astype(jnp.bfloat16)

time: 479 us -> 612 us (1.28)
  waiting for transfers between devices: 219 us -> 347 us
  starting transfers between devices: 45.1 us -> 58.6 us
  blocking collectives: 168 us -> 156 us
    all_gather x2, waiting for transfers between devices: 91.2 us -> 347 us  [sent_together(): lax.all_gather(both, axis, axis=dim, tiled=True)]
    all_gather x1 -> x0, waiting for transfers between devices: 127 us -> none  [on_device(): lax.all_gather(down_weight, 'fs', axis=1, tiled=True)]
    all_to_all x0 -> x1, starting transfers between devices: none -> 13.3 us  [_change_members_all(): lax.all_to_all(jnp.stack([v0] * lax.axis_size('fs'), axis=0), 'fs', 0, 0)]
    all_to_all x2, blocking collectives: 92 us -> 80.3 us  [summed_on_arrival(): tiles = lax.all_to_all(split_up(array, dim, peers), axis, 0, 0, tiled=True)]
  transfers between devices with their start and end apart: 4 -> 4, of which waited for: 3 -> 2; matrix products, arithmetic and copies ran while one was open for 5% -> 2% of each run, Pallas kernels for 0% -> 0%
where the time goes in v1:
time: 612 us; the launch traced here: 611 us
  waiting for transfers between devices  347 us (57%)
  blocking collectives  156 us (25%)
  starting transfers between devices  58.6 us (10%)
  matrix products  20.6 us (3%)
  between operations  13.9 us (2%)
  local copies, waits for them, and re-layouts  7.88 us (1%)
  other arithmetic  7.65 us (1%)
    all_gather x2, waiting for transfers between devices, sent_together(): lax.all_gather(both, axis, axis=dim, tiled=True)  347 us
    all_to_all x2, blocking collectives, summed_on_arrival(): tiles = lax.all_to_all(split_up(array, dim, peers), axis, 0, 0, tiled=True)  80.3 us
    all_gather x1, blocking collectives, on_device(): lax.all_gather(merge_weight, 'fs', axis=1, tiled=True)  51.5 us
    all_to_all x1, starting transfers between devices, copy_for_each(): return lax.all_to_all(copies, axis, split_axis=0, concat_axis=0, tiled=True)  45.1 us
    all_to_all x1, blocking collectives, copy_for_each(): return lax.all_to_all(copies, axis, split_axis=0, concat_axis=0, tiled=True)  24.1 us
    all_to_all x1, starting transfers between devices, _change_members_all(): lax.all_to_all(jnp.stack([v0] * lax.axis_size('fs'), axis=0), 'fs', 0, 0)  13.3 us
  transfers between devices with their start and end apart: 4, of which 2 were waited for; matrix products, arithmetic and copies ran while one was open for 2% of the time, Pallas kernels for 0%

profile of v1, /device:TPU:33, one launch (start us, length us, event | category | flops | bytes accessed | tf_op | source)
XLA Modules:
  0.0 611.3 jit_solution(9799533186737019383)
XLA Ops:
  6.6 1.4 pad_maximum_fusion.2
  8.0 1.1 copy.42
  9.1 1.3 broadcast_in_dim.28
  10.4 45.1 %all-to-all-start = ((bf16[8,1,384,256]{2,3,1,0:T(8,128)(2,1)}), bf16[8,1,384,256]{2,3,1,0:T(8,128)(2,1)S(1)}, u32[]{:S(2)}, u32[]{:S(2)}) async-start(bf16[8,1,384,256]{2,3,1,0:T(8,128)(2,1)} %broadcast_in_dim.28), calls=%async_computation | async-start | bytes 3145728 | tf_op jit(solution)/shard_map/all_to_all | solution.py:27
  56.2 51.5 %all_gather.10 = bf16[128,2048]{0,1:T(8,128)(2,1)} all-gather(bf16[128,64]{0,1:T(8,128)(2,1)S(1)} %copy-done.4), channel_id=1, replica_groups=mesh['grp'=2,'fs'=32,'tp'=8] {'fs'}, dimensions={1}, use_global_device_ids=true | all-gather | bytes 540672 | tf_op jit(solution)/shard_map/all_gather | solution.py:194
  107.7 0.4 multiply_reduce_fusion.1
  108.4 0.5 copy-done.5
  108.9 0.4 fusion.3
  109.2 41.9 %all-gather.3.cloned.1.call-done = bf16[2048,512]{1,0:T(8,128)(2,1)} async-done(((bf16[64,512]{1,0:T(8,128)(2,1)}), bf16[2048,512]{1,0:T(8,128)(2,1)}) %all-gather.3.cloned.1.call-update) | async-done | bytes 2097168 | tf_op jit(solution)/shard_map/all_gather | solution.py:36
  151.2 1.7 convolution_convert_fusion.4
  153.1 1.5 convolution_convert_fusion.3
  154.7 1.5 convolution_convert_fusion.2
  156.7 0.3 while.31
  157.7 0.8 convolution_multiply_fusion
  158.5 0.5 fusion.17
  159.0 0.5 fusion.16
  159.5 0.5 fusion.56
  160.5 0.9 reshape.449
  161.4 0.8 copy.59
  162.2 3.2 convolution_convert_fusion.1
  165.6 45.7 %all_to_all.25 = bf16[8,384,256]{2,1,0:T(8,128)(2,1)S(1)} all-to-all(bf16[8,384,256]{2,1,0:T(8,128)(2,1)S(1)} %bitcast.143), channel_id=1, replica_groups=mesh['grp'=2,'fs'=32,'tp'=8] {'tp'}, dimensions={0} | all-to-all | bytes 3145728 | tf_op jit(solution)/shard_map/all_to_all | solution.py:51
  211.9 24.1 %all_to_all.26 = bf16[8,384,256]{1,2,0:T(8,128)(2,1)S(1)} all-to-all(bf16[8,384,256]{1,2,0:T(8,128)(2,1)S(1)} %broadcast_in_dim.33), channel_id=1, replica_groups=mesh['grp'=2,'fs'=32,'tp'=8] {'tp'}, dimensions={0} | all-to-all | bytes 3145728 | tf_op jit(solution)/shard_map/all_to_all | solution.py:27
  236.0 1.9 stack.2
  237.9 13.3 %all-to-all-start.3 = ((bf16[32,640,64]{1,2,0:T(8,128)(2,1)}), bf16[32,640,64]{1,2,0:T(8,128)(2,1)}, u32[]{:S(2)}, u32[]{:S(2)}) async-start(bf16[32,640,64]{1,2,0:T(8,128)(2,1)} %stack.2), calls=%async_computation.3 | async-start | bytes 5242880 | tf_op jit(solution)/shard_map/all_to_all | solution.py:15
  251.5 0.7 pad_maximum_fusion.1
  252.2 0.4 multiply_reduce_fusion
  252.7 1.6 fusion.1
  254.3 304.6 %all-gather.5.cloned.1.call-done = bf16[2048,1280]{1,0:T(8,128)(2,1)} async-done(((bf16[64,1280]{1,0:T(8,128)(2,1)}), bf16[2048,1280]{1,0:T(8,128)(2,1)}) %all-gather.5.cloned.1.call-update) | async-done | bytes 5242896 | tf_op jit(solution)/shard_map/all_gather | solution.py:36
  558.9 3.6 fusion.6
  562.5 6.2 %convolution_convert_fusion = bf16[384,2048]{1,0:T(8,128)(2,1)S(1)} fusion(bf16[640,2048]{0,1:T(8,128)(2,1)} %bitcast.31, bf16[384,2048]{0,1:T(8,128)(2,1)} %fusion.1, bf16[2048,1280]{1,0:T(8,128)(2,1)} %all-gather.5.cloned.1.call-done, f32[384,640]{1,0:T(8,128)S(1)} %fusion.6), kind=kOutput, calls=%fused_computation.14 | convolution fusion | flops 2015526912 | bytes 9371648 | tf_op jit(solution)/shard_map/dot_general | solution.py:207
  568.8 34.6 %all_to_all.27 = bf16[8,384,256]{2,1,0:T(8,128)(2,1)S(1)} all-to-all(bf16[8,384,256]{2,1,0:T(8,128)(2,1)S(1)} %bitcast.144), channel_id=1, replica_groups=mesh['grp'=2,'fs'=32,'tp'=8] {'tp'}, dimensions={0} | all-to-all | bytes 3145728 | tf_op jit(solution)/shard_map/all_to_all | solution.py:51
  603.7 0.7 fusion.26
  (80 shorter events, 4.6 us)
Async XLA Ops:
  6.5 144.6 %all-gather.3.cloned.1.call-start = ((), (), s32[]{:S(2)}) async-start(), calls=%async_computation.5 | async-start | bytes 2162688 | tf_op jit(solution)/shard_map/all_gather | solution.py:36
  9.1 46.5 %copy-start.7 = (f32[2]{0:T(128)S(1)}, f32[2]{0:T(128)}, u32[]{:S(2)}) copy-start(f32[2]{0:T(128)} %param.24) | copy-start | bytes 28
  9.1 46.5 %copy-start.8 = (f32[2]{0:T(128)S(1)}, f32[2]{0:T(128)}, u32[]{:S(2)}) copy-start(f32[2]{0:T(128)} %param.23) | copy-start | bytes 28
  10.4 45.8 %copy-start.4 = (bf16[128,64]{0,1:T(8,128)(2,1)S(1)}, bf16[128,64]{0,1:T(8,128)(2,1)}, u32[]{:S(2)}) copy-start(bf16[128,64]{0,1:T(8,128)(2,1)} %param.25) | copy-start | bytes 49156
  10.4 97.3 %all-to-all-start = ((bf16[8,1,384,256]{2,3,1,0:T(8,128)(2,1)}), bf16[8,1,384,256]{2,3,1,0:T(8,128)(2,1)S(1)}, u32[]{:S(2)}, u32[]{:S(2)}) async-start(bf16[8,1,384,256]{2,3,1,0:T(8,128)(2,1)} %broadcast_in_dim.28), calls=%async_computation | async-start | bytes 3145728 | tf_op jit(solution)/shard_map/all_to_all | solution.py:27
  108.2 0.7 copy-start.5
  165.6 46.0 %copy-start = (bf16[1,384,256]{2,1,0:T(8,128)(2,1)S(1)}, bf16[1,384,256]{2,1,0:T(8,128)(2,1)}, u32[]{:S(2)}) copy-start(bf16[1,384,256]{2,1,0:T(8,128)(2,1)} %param.17) | copy-start | bytes 589828
  211.8 24.3 %copy-start.3 = (bf16[640,64]{0,1:T(8,128)(2,1)S(1)}, bf16[640,64]{0,1:T(8,128)(2,1)}, u32[]{:S(2)}) copy-start(bf16[640,64]{0,1:T(8,128)(2,1)} %param.29) | copy-start | bytes 245764
  237.9 13.6 %copy-start.1 = (bf16[64,640]{1,0:T(8,128)(2,1)S(1)}, bf16[64,640]{1,0:T(8,128)(2,1)}, u32[]{:S(2)}) copy-start(bf16[64,640]{1,0:T(8,128)(2,1)} %param.28) | copy-start | bytes 245764
  237.9 13.6 %copy-start.2 = (bf16[64,640]{1,0:T(8,128)(2,1)S(1)}, bf16[64,640]{1,0:T(8,128)(2,1)}, u32[]{:S(2)}) copy-start(bf16[64,640]{1,0:T(8,128)(2,1)} %param.27) | copy-start | bytes 245764
  237.9 14.7 %copy-start.6 = (f32[2048]{0:T(1024)S(1)}, f32[2048]{0:T(1024)}, u32[]{:S(2)}) copy-start(f32[2048]{0:T(1024)} %param.26) | copy-start | bytes 24580
  237.9 324.6 %all-to-all-start.3 = ((bf16[32,640,64]{1,2,0:T(8,128)(2,1)}), bf16[32,640,64]{1,2,0:T(8,128)(2,1)}, u32[]{:S(2)}, u32[]{:S(2)}) async-start(bf16[32,640,64]{1,2,0:T(8,128)(2,1)} %stack.2), calls=%async_computation.3 | async-start | bytes 5242880 | tf_op jit(solution)/shard_map/all_to_all | solution.py:15
  251.2 307.6 %all-gather.5.cloned.1.call-start = ((), (), s32[]{:S(2)}) async-start(), calls=%async_computation.6 | async-start | bytes 5406720 | tf_op jit(solution)/shard_map/all_gather | solution.py:36
Sparse Core Ops, SparseCore 0:
  9.4 141.6 all-gather.2
  254.2 304.6 all-gather.4
